TPU v7x, 32 devices: a whole 2x2x4 slice. The times are simulated.
32 devices in a mesh: rep: 8 (over z, y), fs: 2 (over core), tp: 2 (over x).
Axes of the slice: x: 2, y: 2, z: 4, core: 2. Of those that a mesh axis runs over, the one named last changes fastest.
Arguments:
- inputs: bfloat16 [2048, 2048], P(('rep', 'fs'), 'tp'), may hold values from -6 to 6
- cotangent: bfloat16 [2048, 2048], P(('rep', 'fs'), 'tp'), may hold values from -6 to 6
- w_up: bfloat16 [2048, 4096], P('fs', 'tp'), may hold values from -0.125 to 0.125
- w_down: bfloat16 [4096, 2048], P('tp', 'fs'), may hold values from -0.09375 to 0.09375
Outputs:
- grad_inputs: bfloat16 [2048, 2048], P(('rep', 'fs'), 'tp')
- grad_up: float32 [2048, 4096], P('fs', 'tp')
- grad_down: float32 [4096, 2048], P('tp', 'fs')
All inputs are finite; a program needn't handle non-finite values.
Results may differ from a plain program's by a relative error of at most 0.011.
Values may be sent and summed in bfloat16 or wider, within the bound.
A program may use at most 128 MiB of HBM per device.

v0:
```python
import jax
import jax.numpy as jnp
from jax import lax
from jax.sharding import PartitionSpec as P


def contract_rows(left, right):
    return lax.dot_general(
        left, right, (((0,), (0,)), ((), ())), preferred_element_type=jnp.float32
    )


def contract_cols(left, right):
    return lax.dot_general(
        left, right, (((1,), (1,)), ((), ())), preferred_element_type=jnp.float32
    )


def shards(inputs, cotangent, w_up, w_down):
    rows_in, rows_cot = (
        lax.all_gather(inputs, "tp", axis=1, tiled=True),
        lax.all_gather(cotangent, "tp", axis=1, tiled=True),
    )
    cols_in, cols_cot = (
        lax.all_to_all(rows_in, "fs", split_axis=1, concat_axis=0, tiled=True),
        lax.all_to_all(rows_cot, "fs", split_axis=1, concat_axis=0, tiled=True),
    )
    full_up, full_down = (
        lax.all_gather(w_up, "fs", axis=0, tiled=True),
        lax.all_gather(w_down, "fs", axis=1, tiled=True),
    )
    act_grad = contract_cols(rows_cot, full_down)
    preact = jnp.dot(rows_in, full_up, preferred_element_type=jnp.float32)
    relu_pre = jnp.maximum(preact, 0.0)
    squared = (relu_pre * relu_pre).astype(jnp.bfloat16)
    pre_grad = (2.0 * relu_pre * act_grad).astype(jnp.bfloat16)
    partial_value = contract_cols(pre_grad, full_up)
    grad_inputs = lax.psum_scatter(
        partial_value.astype(jnp.bfloat16), "tp", scatter_dimension=1, tiled=True
    )
    grad_piece = lax.all_gather(pre_grad, "fs", axis=0, tiled=True)
    square_piece = lax.all_gather(squared, "fs", axis=0, tiled=True)
    local_up = contract_rows(cols_in, grad_piece)
    local_down = contract_rows(square_piece, cols_cot)
    slice_up = lax.psum_scatter(local_up, "rep", scatter_dimension=0, tiled=True)
    slice_down = lax.psum_scatter(local_down, "rep", scatter_dimension=0, tiled=True)
    grad_up = lax.all_gather(slice_up, "rep", axis=0, tiled=True)
    grad_down = lax.all_gather(slice_down, "rep", axis=0, tiled=True)
    return (grad_inputs, grad_up, grad_down)


def solution(mesh):
    return jax.shard_map(
        shards,
        mesh=mesh,
        in_specs=(P(("rep", "fs"), "tp"), P(("rep", "fs"), "tp"), P("fs", "tp"), P("tp", "fs")),
        out_specs=(P(("rep", "fs"), "tp"), P("fs", "tp"), P("tp", "fs")),
        check_vma=False,
    )
```

profile of v0, /device:TPU:0, one launch (start us, length us, event | category | flops | bytes accessed | tf_op | source)
XLA Modules:
  0.0 669.8 jit_solution(12744969202771830542)
XLA Ops:
  7.2 0.7 all-gather.7.cloned.1.call-update
  8.0 0.7 all-gather.9.cloned.1.call-update
  8.7 0.0 all-gather.11.cloned.1.call-start
  8.7 0.2 copy.9
  8.9 0.2 copy.10
  9.1 9.9 %all_gather.24 = bf16[128,2048]{0,1:T(8,128)(2,1)S(1)} all-gather(bf16[128,1024]{0,1:T(8,128)(2,1)S(1)} %copy.9), channel_id=1, replica_groups=mesh['rep'=8,'fs'=2,'tp'=2] {'tp'}, dimensions={1}, use_global_device_ids=true | all-gather | bytes 786432 | tf_op jit(solution)/shard_map/all_gather | solution.py:21
  19.0 8.1 %all_gather.26 = bf16[128,2048]{0,1:T(8,128)(2,1)S(1)} all-gather(bf16[128,1024]{0,1:T(8,128)(2,1)S(1)} %copy.10), channel_id=1, replica_groups=mesh['rep'=8,'fs'=2,'tp'=2] {'tp'}, dimensions={1}, use_global_device_ids=true | all-gather | bytes 786432 | tf_op jit(solution)/shard_map/all_gather | solution.py:22
  27.1 5.0 all-gather.7.cloned.1.call-done
  32.1 5.5 multiply_convert_fusion
  37.6 17.1 %all-gather.9.cloned.1.call-done = bf16[2048,2048]{1,0:T(8,128)(2,1)} async-done(((bf16[2048,1024]{1,0:T(8,128)(2,1)}), bf16[2048,2048]{1,0:T(8,128)(2,1)}) %all-gather.9.cloned.1.call-update) | async-done | bytes 8388624 | tf_op jit(solution)/shard_map/all_gather | solution.py:30
  54.7 7.1 %fusion = bf16[128,2048]{1,0:T(8,128)(2,1)} fusion(bf16[128,2048]{0,1:T(8,128)(2,1)S(1)} %all_gather.26, bf16[2048,2048]{1,0:T(8,128)(2,1)} %all-gather.9.cloned.1.call-done, f32[128,2048]{1,0:T(8,128)S(1)} %get-tuple-element.13), kind=kOutput, calls=%fused_computation.4 | convolution fusion | flops 1074528256 | bytes 10485760 | tf_op jit(solution)/shard_map/dot_general | solution.py:14
  61.9 0.0 all-gather.15.cloned.1.call-start
  61.9 0.5 all-gather.15.cloned.1.call-update
  62.4 0.0 reduce-scatter.6.cloned.1.call-start
  62.5 4.2 all_to_all.38
  66.6 0.2 copy.11
  66.9 5.4 all-gather.11.cloned.1.call-done
  72.2 5.9 convolution_bitcast_fusion
  78.2 0.0 reduce-scatter.8.cloned.1.call-start
  78.2 4.2 all_to_all.39
  82.4 0.2 copy.12
  82.6 1.9 all-gather.15.cloned.1.call-done
  84.4 6.0 fusion.1
  90.4 0.0 all-gather.13.cloned.1.call-start
  90.5 147.1 %reduce-scatter.6.cloned.1.call-done = f32[128,2048]{0,1:T(8,128)} async-done(((f32[1024,2048]{0,1:T(8,128)}), f32[128,2048]{0,1:T(8,128)}) %reduce-scatter.6.cloned.1.call-update) | async-done | bytes 1048592 | tf_op jit(solution)/shard_map/reduce_scatter | solution.py:45
  237.6 150.6 %reduce-scatter.8.cloned.1.call-done = f32[256,1024]{1,0:T(8,128)} async-done(((f32[2048,1024]{1,0:T(8,128)}), f32[256,1024]{1,0:T(8,128)}) %reduce-scatter.8.cloned.1.call-update) | async-done | bytes 1048592 | tf_op jit(solution)/shard_map/reduce_scatter | solution.py:46
  388.3 7.1 %convolution_convert_fusion = bf16[128,2048]{1,0:T(8,128)(2,1)} fusion(bf16[128,2048]{1,0:T(8,128)(2,1)S(1)} %copy-done, bf16[2048,2048]{1,0:T(8,128)(2,1)} %all-gather.7.cloned.1.call-done), kind=kOutput, calls=%fused_computation.3 | convolution fusion | flops 1074003968 | bytes 9437184 | tf_op jit(solution)/shard_map/dot_general | solution.py:14
  395.4 118.9 %all-gather.13.cloned.1.call-done = f32[1024,2048]{0,1:T(8,128)} async-done(((f32[128,2048]{0,1:T(8,128)}), f32[1024,2048]{0,1:T(8,128)}) %all-gather.13.cloned.1.call-update) | async-done | bytes 8388624 | tf_op jit(solution)/shard_map/all_gather | solution.py:47
  514.3 9.2 %copy.13 = f32[1024,2048]{1,0:T(8,128)} copy(f32[1024,2048]{0,1:T(8,128)} %all-gather.13.cloned.1.call-done) | data formatting | bytes 16777216
  523.5 115.6 %all-gather.17.cloned.1.call-done = f32[2048,1024]{1,0:T(8,128)} async-done(((f32[256,1024]{1,0:T(8,128)}), f32[2048,1024]{1,0:T(8,128)}) %all-gather.17.cloned.1.call-update) | async-done | bytes 8388624 | tf_op jit(solution)/shard_map/all_gather | solution.py:48
  639.1 15.6 %reduce-scatter.4.cloned.1.call-done = bf16[128,1024]{1,0:T(8,128)(2,1)} async-done(((bf16[128,2048]{1,0:T(8,128)(2,1)}), bf16[128,1024]{1,0:T(8,128)(2,1)}) %reduce-scatter.4.cloned.1.call-update) | async-done | bytes 262160 | tf_op jit(solution)/shard_map/reduce_scatter | solution.py:38
  654.8 8.4 %copy.15 = f32[2048,1024]{1,0:T(8,128)} copy(f32[2048,1024]{1,0:T(8,128)} %all-gather.17.cloned.1.call-done) | data formatting | bytes 16777216
  (16 shorter events, 0.3 us)
Async XLA Ops:
  7.2 1.6 copy-start.1
  7.2 1.7 copy-start.2
  7.2 25.0 %all-gather.7.cloned.1.call-start = ((), (), s32[]{:S(2)}) async-start(), calls=%async_computation.5 | async-start | bytes 12582912 | tf_op jit(solution)/shard_map/all_gather | solution.py:29
  7.9 46.8 %all-gather.9.cloned.1.call-start = ((), (), s32[]{:S(2)}) async-start(), calls=%async_computation.6 | async-start | bytes 12582912 | tf_op jit(solution)/shard_map/all_gather | solution.py:30
  8.7 63.6 %all-gather.11.cloned.1.call-start = ((), (), s32[]{:S(2)}) async-start(), calls=%async_computation.8 | async-start | bytes 1572864 | tf_op jit(solution)/shard_map/all_gather | solution.py:41
  61.9 22.6 %all-gather.15.cloned.1.call-start = ((), (), s32[]{:S(2)}) async-start(), calls=%async_computation.11 | async-start | bytes 1572864 | tf_op jit(solution)/shard_map/all_gather | solution.py:42
  62.4 175.1 %reduce-scatter.6.cloned.1.call-start = ((), (), s32[]{:S(2)}) async-start(), calls=%async_computation.9 | async-start | bytes 9437184 | tf_op jit(solution)/shard_map/reduce_scatter | solution.py:45
  78.2 310.1 %reduce-scatter.8.cloned.1.call-start = ((), (), s32[]{:S(2)}) async-start(), calls=%async_computation.12 | async-start | bytes 9437184 | tf_op jit(solution)/shard_map/reduce_scatter | solution.py:46
  84.4 303.9 %copy-start = (bf16[128,2048]{1,0:T(8,128)(2,1)S(1)}, bf16[128,2048]{1,0:T(8,128)(2,1)}, u32[]{:S(2)}) copy-start(bf16[128,2048]{1,0:T(8,128)(2,1)} %fusion) | copy-start | bytes 1572868
  90.4 423.9 %all-gather.13.cloned.1.call-start = ((), (), s32[]{:S(2)}) async-start(), calls=%async_computation.10 | async-start | bytes 9437184 | tf_op jit(solution)/shard_map/all_gather | solution.py:47
  237.6 401.6 %all-gather.17.cloned.1.call-start = ((), (), s32[]{:S(2)}) async-start(), calls=%async_computation.13 | async-start | bytes 9437184 | tf_op jit(solution)/shard_map/all_gather | solution.py:48
  388.2 266.5 %reduce-scatter.4.cloned.1.call-start = ((), (), s32[]{:S(2)}) async-start(), calls=%async_computation.7 | async-start | bytes 786432 | tf_op jit(solution)/shard_map/reduce_scatter | solution.py:38
Sparse Core Ops, SparseCore 0:
  9.5 22.5 all-gather.6
  33.7 21.0 all-gather.8
  62.0 10.1 all-gather.10
  74.2 10.1 all-gather.14
  88.5 149.0 reduce-scatter.5
  241.6 146.5 reduce-scatter.7
  390.3 124.0 all-gather.12
  516.5 122.6 all-gather.16
  642.0 12.7 reduce-scatter.3
where the time goes:
time: 670 us
  waiting for transfers between devices  579 us (86%)
  matrix products  31.5 us (5%)
  blocking collectives  26.4 us (4%)
  local copies, waits for them, and re-layouts  18.4 us (3%)
  between operations  13.9 us (2%)
    reduce_scatter x1, waiting for transfers between devices, shards(): lax.psum_scatter(local_down, 'rep', scatter_dimension=0, tiled=True)  151 us
    reduce_scatter x1, waiting for transfers between devices, shards(): lax.psum_scatter(local_up, 'rep', scatter_dimension=0, tiled=True)  147 us
    all_gather x1, waiting for transfers between devices, shards(): grad_up = lax.all_gather(slice_up, 'rep', axis=0, tiled=True)  119 us
    all_gather x1, waiting for transfers between devices, shards(): grad_down = lax.all_gather(slice_down, 'rep', axis=0, tiled=True)  116 us
    unnamed x10, local copies, waits for them, and re-layouts  18 us
    all_gather x1, waiting for transfers between devices, shards(): lax.all_gather(w_down, 'fs', axis=1, tiled=True)  17.1 us
    reduce_scatter x1, waiting for transfers between devices, shards(): lax.psum_scatter(partial_value.astype(jnp.bfloat16), 'tp', scatter_dimens...  15.6 us
    dot_general x2, matrix products, contract_cols(): lax.dot_general(left, right, (((1,), (1,)), ((), ())), preferred_element_...  14.2 us
  transfers between devices with their start and end apart: 9, of which 9 were waited for; matrix products, arithmetic and copies ran while one was open for 5% of the time, Pallas kernels for 0%

commit v1 on v0

--- a/solution.py
+++ b/solution.py
@@ -1,7 +1,15 @@
+import functools
+
 import jax
 import jax.numpy as jnp
 from jax import lax
+from jax.experimental import pallas as pl
+from jax.experimental.pallas import tpu as pltpu
 from jax.sharding import PartitionSpec as P
+
+MESH = pl.DeviceIdType.MESH
+X, Y, UP, DOWN = range(4)
+PAIR = 2
 
 
 def contract_rows(left, right):
@@ -16,7 +24,205 @@
     )
 
 
-def shards(inputs, cotangent, w_up, w_down):
+def gather_kernel(reps, x_ref, c_ref, up_ref, down_ref, gx, gc, up_other, down_other,
+                  send_sem, recv_sem, swap_sem, own_sem):
+    rep, fs, tp = lax.axis_index("rep"), lax.axis_index("fs"), lax.axis_index("tp")
+    z, y = rep // PAIR, rep % PAIR
+    depth = reps // PAIR
+    half = x_ref.shape[0] // 2
+    target = {
+        X: {"tp": 1 - tp},
+        Y: {"rep": z * PAIR + (1 - y)},
+        UP: {"rep": jnp.minimum(z + 1, depth - 1) * PAIR + y},
+        DOWN: {"rep": jnp.maximum(z - 1, 0) * PAIR + y},
+    }
+    sibling = {"fs": 1 - fs}
+
+    def when(condition, body):
+        if condition is True:
+            body()
+        else:
+            pl.when(condition)(body)
+
+    barrier = pltpu.get_barrier_semaphore()
+
+    def greet(device):
+        pl.semaphore_signal(barrier, inc=1, device_id=device, device_id_type=MESH)
+
+    greet(target[X])
+    greet(target[Y])
+    greet(sibling)
+    when(z < depth - 1, lambda: greet(target[UP]))
+    when(z > 0, lambda: greet(target[DOWN]))
+    pl.semaphore_wait(barrier, 3 + (z < depth - 1).astype(jnp.int32) + (z > 0).astype(jnp.int32))
+
+    def copy(way, sub, at, own=False):
+        at_z, at_y, at_t = at
+        array, part = sub
+        rows = pl.ds(part * half, half)
+        source = at_z * PAIR + at_y
+        slot = (at_t + fs) % 2
+        there = (gx, gc)[array].at[slot, source, rows]
+        here = (x_ref, c_ref)[array].at[rows] if own else there
+        index, piece = array * 2 + part, source * 2 + at_t
+        return pltpu.make_async_remote_copy(
+            src_ref=here, dst_ref=there,
+            send_sem=send_sem.at[way, index, piece],
+            recv_sem=recv_sem.at[index, piece],
+            device_id=target[way], device_id_type=MESH,
+        )
+
+    started = []
+
+    def start(way, sub, at, condition=True, own=False):
+        when(condition, lambda: copy(way, sub, at, own).start())
+        started.append((way, sub, at, condition, own))
+
+    def arrive(sub, at, condition=True):
+        when(condition, lambda: copy(X, sub, at).wait_recv())
+
+    subs = [(array, part) for part in range(2) for array in range(2)]
+    first = [(array, 0) for array in range(2)]
+    second = [(array, 1) for array in range(2)]
+
+    swaps = [
+        pltpu.make_async_remote_copy(
+            src_ref=mine, dst_ref=theirs, send_sem=swap_sem.at[0, index], recv_sem=swap_sem.at[1, index],
+            device_id=sibling, device_id_type=MESH,
+        )
+        for index, (mine, theirs) in enumerate(((up_ref, up_other), (down_ref, down_other)))
+    ]
+
+    here = (z, y, tp)
+    for sub in subs:
+        start(UP, sub, here, z < depth - 1, own=True)
+        start(DOWN, sub, here, z > 0, own=True)
+    for sub in first + second:
+        start(X, sub, here, own=True)
+    for sub in second + first:
+        start(Y, sub, here, own=True)
+    for swap in swaps:
+        swap.start()
+    owns = [
+        pltpu.make_async_copy(mine, whole.at[(tp + fs) % 2, rep], own_sem.at[index])
+        for index, (mine, whole) in enumerate(((x_ref, gx), (c_ref, gc)))
+    ]
+    for own in owns:
+        own.start()
+
+    def planes(step):
+        if step == 0:
+            return [(z, True, None, None)]
+        return [
+            (jnp.maximum(z - step, 0), z - step >= 0, UP, z < depth - 1),
+            (jnp.minimum(z + step, depth - 1), z + step < depth, DOWN, z > 0),
+        ]
+
+    def both(one, other):
+        return other if one is True else jnp.logical_and(one, other)
+
+    def from_z(step):
+        for at_z, there, way, more in planes(step):
+            at = (at_z, y, tp)
+            for sub in subs:
+                arrive(sub, at, there)
+                if step < depth - 1:
+                    start(way, sub, at, both(there, more))
+            for sub in first + second:
+                start(X, sub, at, there)
+            for sub in second + first:
+                start(Y, sub, at, there)
+
+    def cross(step):
+        for at_z, there, _, _ in planes(step):
+            for one, two in zip(first, second):
+                across_x, across_y = (at_z, y, 1 - tp), (at_z, 1 - y, tp)
+                arrive(one, across_x, there)
+                start(Y, one, across_x, there)
+                arrive(two, across_y, there)
+                start(X, two, across_y, there)
+
+    def rest(step):
+        for at_z, there, _, _ in planes(step):
+            for one, two in zip(first, second):
+                arrive(one, (at_z, 1 - y, tp), there)
+                arrive(two, (at_z, y, 1 - tp), there)
+            for sub in subs:
+                arrive(sub, (at_z, 1 - y, 1 - tp), there)
+
+    cross(0)
+    for step in range(1, depth):
+        from_z(step)
+        if step >= 2:
+            cross(step - 1)
+    if depth > 1:
+        cross(depth - 1)
+    for step in range(depth):
+        rest(step)
+    for own in owns:
+        own.wait()
+    for swap in swaps:
+        swap.wait()
+    for way, sub, at, condition, own in started:
+        when(condition, lambda: copy(way, sub, at, own).wait_send())
+
+
+def gather_all(reps, inputs, cotangent, w_up, w_down):
+    rows, cols = inputs.shape
+    whole = jax.ShapeDtypeStruct((2, reps, rows, cols), inputs.dtype)
+    anywhere, vmem = pl.BlockSpec(memory_space=pl.ANY), pl.BlockSpec(memory_space=pltpu.VMEM)
+    return pl.pallas_call(
+        functools.partial(gather_kernel, reps),
+        out_shape=(
+            whole, whole,
+            jax.ShapeDtypeStruct(w_up.shape, w_up.dtype), jax.ShapeDtypeStruct(w_down.shape, w_down.dtype),
+        ),
+        in_specs=[vmem, vmem, anywhere, anywhere],
+        out_specs=[anywhere] * 4,
+        scratch_shapes=[
+            pltpu.SemaphoreType.DMA((4, 4, reps * 2)),
+            pltpu.SemaphoreType.DMA((4, reps * 2)),
+            pltpu.SemaphoreType.DMA((2, 2)),
+            pltpu.SemaphoreType.DMA((2,)),
+        ],
+        compiler_params=pltpu.CompilerParams(collective_id=0, has_side_effects=True),
+    )(inputs, cotangent, w_up, w_down)
+
+
+def swapped(value, axis):
+    return lax.ppermute(value, axis, [(0, 1), (1, 0)])
+
+
+def few_tokens(reps, inputs, cotangent, w_up, w_down):
+    rows = inputs.shape[0]
+    rep, fs, tp = lax.axis_index("rep"), lax.axis_index("fs"), lax.axis_index("tp")
+    gx, gc, up_other, down_other = gather_all(reps, inputs, cotangent, w_up, w_down)
+    gx, gc = (value.reshape(2, -1, value.shape[-1]) for value in (gx, gc))
+    preact = (
+        jnp.dot(gx[0], w_up, preferred_element_type=jnp.float32)
+        + jnp.dot(gx[1], up_other, preferred_element_type=jnp.float32)
+    )
+    act_grad = contract_cols(gc[0], w_down) + contract_cols(gc[1], down_other)
+    relu_pre = jnp.maximum(preact, 0.0)
+    squared = (relu_pre * relu_pre).astype(jnp.bfloat16)
+    pre_grad = (2.0 * relu_pre * act_grad).astype(jnp.bfloat16)
+
+    own_rows = lax.dynamic_slice_in_dim(pre_grad, rep * rows, rows, 0)
+    part_own = contract_cols(own_rows, w_up).astype(jnp.bfloat16)
+    part_other = contract_cols(own_rows, up_other).astype(jnp.bfloat16)
+    same = fs == tp
+    mine = jnp.where(same, part_own, part_other)
+    theirs = swapped(jnp.where(same, part_other, part_own), "tp")
+
+    up_theirs = swapped(contract_rows(gx[1], pre_grad).astype(jnp.bfloat16), "fs")
+    down_theirs = swapped(contract_rows(squared, gc[1]).astype(jnp.bfloat16), "fs")
+    grad_up = contract_rows(gx[0], pre_grad) + up_theirs.astype(jnp.float32)
+    grad_down = contract_rows(squared, gc[0]) + down_theirs.astype(jnp.float32)
+    grad_inputs = (mine.astype(jnp.float32) + theirs.astype(jnp.float32)).astype(jnp.bfloat16)
+    return grad_inputs, grad_up, grad_down
+
+
+def many_tokens(inputs, cotangent, w_up, w_down):
     rows_in, rows_cot = (
         lax.all_gather(inputs, "tp", axis=1, tiled=True),
         lax.all_gather(cotangent, "tp", axis=1, tiled=True),
@@ -50,6 +256,16 @@
 
 
 def solution(mesh):
+    reps, n_fs, n_tp = mesh.shape["rep"], mesh.shape["fs"], mesh.shape["tp"]
+
+    def shards(inputs, cotangent, w_up, w_down):
+        gathered = 2 * reps * n_tp * inputs.size * inputs.dtype.itemsize
+        gradients = (w_up.size + w_down.size) * 4
+        fits = n_fs == 2 and n_tp == 2 and reps % PAIR == 0 and inputs.shape[0] % 32 == 0
+        if fits and gathered <= gradients:
+            return few_tokens(reps, inputs, cotangent, w_up, w_down)
+        return many_tokens(inputs, cotangent, w_up, w_down)
+
     return jax.shard_map(
         shards,
         mesh=mesh,

time: 670 us -> 157 us (0.23)
  waiting for transfers between devices: 579 us -> 6.94 us
  Pallas kernels: 0 us -> 76.6 us
  matrix products: 31.5 us -> 65.6 us
  blocking collectives: 26.4 us -> 0 us
  local copies, waits for them, and re-layouts: 18.4 us -> 4.67 us
  between operations: 13.9 us -> 0.76 us
    reduce_scatter x3 -> x0, waiting for transfers between devices: 313 us -> none  [the longest x1 151 us: shards(): lax.psum_scatter(local_down, 'rep', scatter_dimension=0, tiled=True)]
    all_gather x6 -> x0, waiting for transfers between devices: 264 us -> none  [the longest x1 119 us: shards(): grad_up = lax.all_gather(slice_up, 'rep', axis=0, tiled=True)]
    pallas_call x0 -> x1, Pallas kernels: none -> 76.6 us  [gather_all(): pl.pallas_call(functools.partial(gather_kernel, reps), out_shape=(whole,...]
    dot_general x2 -> x4, matrix products: 11.9 us -> 30.2 us  [contract_rows(): lax.dot_general(left, right, (((0,), (0,)), ((), ())), preferred_element_...]
    all_gather x2 -> x0, blocking collectives: 18.1 us -> none  [the longest x1 9.94 us: shards(): lax.all_gather(inputs, 'tp', axis=1, tiled=True)]
    unnamed x10 -> x20, local copies, waits for them, and re-layouts: 18 us -> 0.6 us
    dot_general x2 -> x4, matrix products: 14.2 us -> 24.1 us  [contract_cols(): lax.dot_general(left, right, (((1,), (1,)), ((), ())), preferred_element_...]
    all_to_all x2 -> x0, blocking collectives: 8.31 us -> none  [the longest x1 4.15 us: shards(): lax.all_to_all(rows_cot, 'fs', split_axis=1, concat_axis=0, tiled=True)]
  transfers between devices with their start and end apart: 9 -> 3, of which waited for: 9 -> 1; matrix products, arithmetic and copies ran while one was open for 5% -> 15% of each run, Pallas kernels for 0% -> 0%
where the time goes in v1:
time: 157 us
  Pallas kernels  76.6 us (49%)
  matrix products  65.6 us (42%)
  waiting for transfers between devices  6.94 us (4%)
  local copies, waits for them, and re-layouts  4.67 us (3%)
  starting transfers between devices  1.85 us (1%)
    pallas_call x1, Pallas kernels, gather_all(): pl.pallas_call(functools.partial(gather_kernel, reps), out_shape=(whole,...  76.6 us
    dot_general x4, matrix products, contract_rows(): lax.dot_general(left, right, (((0,), (0,)), ((), ())), preferred_element_...  30.2 us
    dot_general x4, matrix products, contract_cols(): lax.dot_general(left, right, (((1,), (1,)), ((), ())), preferred_element_...  24.1 us
    ppermute x3, waiting for transfers between devices, swapped(): return lax.ppermute(value, axis, [(0, 1), (1, 0)])  6.94 us
    dot_general x1, matrix products, few_tokens(): jnp.dot(gx[1], up_other, preferred_element_type=jnp.float32)  6.81 us
    dot_general x1, matrix products, few_tokens(): jnp.dot(gx[0], w_up, preferred_element_type=jnp.float32)  4.54 us
    slice x1, local copies, waits for them, and re-layouts, few_tokens(): act_grad = contract_cols(gc[0], w_down) + contract_cols(gc[1], down_other)  4.07 us
  transfers between devices with their start and end apart: 3, of which 1 were waited for; matrix products, arithmetic and copies ran while one was open for 15% of the time, Pallas kernels for 0%

profile of v1, /device:TPU:0, one launch (start us, length us, event | category | flops | bytes accessed | tf_op | source)
XLA Modules:
  0.0 157.3 jit_solution(16468450075336346009)
XLA Ops:
  0.6 76.6 %shard_map.67 = (bf16[2,8,128,1024]{3,2,1,0:T(8,128)(2,1)}, bf16[2,8,128,1024]{3,2,1,0:T(8,128)(2,1)}, bf16[1024,2048]{1,0:T(8,128)(2,1)}, bf16[2048,1024]{1,0:T(8,128)(2,1)}) custom-call(bf16[128,1024]{1,0:T(8,128)(2,1)} %x_ref.1, bf16[128,1024]{1,0:T(8,128)(2,1)} %c_ref.1, bf16[1024,2048]{1,0:T(8,128)(2,1)} %up_ref.1, bf16[2048,1024]{1,0:T(8,128)(2,1)} %down_ref.1), custom_call_target="tpu_custom_call" | custom-call | tf_op jit(solution)/shard_map/pallas_call | solution.py:174
  77.2 0.0 copy-start.3
  77.3 4.1 %fusion.5 = (bf16[1,8,128,1024]{3,2,1,0:T(8,128)(2,1)S(1)}, bf16[1,8,128,1024]{3,2,1,0:T(8,128)(2,1)S(1)}, bf16[1,8,128,1024]{3,2,1,0:T(8,128)(2,1)S(1)}, bf16[1,8,128,1024]{3,2,1,0:T(8,128)(2,1)S(1)}) fusion(bf16[2,8,128,1024]{3,2,1,0:T(8,128)(2,1)} %get-tuple-element.9, bf16[2,8,128,1024]{3,2,1,0:T(8,128)(2,1)} %get-tuple-element.7), kind=kLoop, calls=%fused_computation.16 | loop fusion | bytes 16777216 | tf_op jit(solution)/shard_map/slice | solution.py:205
  81.3 0.0 copy-start.5
  81.3 0.6 copy-done.3
  81.9 6.8 %fusion.8 = f32[1024,2048]{1,0:T(8,128)} fusion(bf16[1024,1024]{1,0:T(8,128)(2,1)S(1)} %bitcast.22, bf16[2048,1024]{1,0:T(8,128)(2,1)S(1)} %copy-done.3), kind=kOutput, calls=%fused_computation.19 | convolution fusion | flops 4294967296 | bytes 14680064 | tf_op jit(solution)/shard_map/dot_general | solution.py:22
  88.7 0.0 copy-done.5
  88.7 0.0 copy-done
  88.7 4.5 %fusion.7 = f32[1024,2048]{1,0:T(8,128)S(1)} fusion(bf16[1024,1024]{1,0:T(8,128)(2,1)S(1)} %bitcast.20, bf16[1024,2048]{1,0:T(8,128)(2,1)S(1)} %copy-done), kind=kOutput, calls=%fused_computation.18 | convolution fusion | flops 4294967296 | bytes 14680064 | tf_op jit(solution)/shard_map/dot_general | solution.py:202
  93.2 0.0 copy-done.4
  93.2 6.8 %add_maximum_fusion = f32[1024,2048]{1,0:T(8,128)} fusion(f32[1024,2048]{1,0:T(8,128)S(1)} %fusion.7, bf16[1024,1024]{1,0:T(8,128)(2,1)S(1)} %bitcast.26, bf16[1024,2048]{1,0:T(8,128)(2,1)S(1)} %copy-done.4), kind=kOutput, calls=%fused_computation.4 | convolution fusion | flops 4299161600 | bytes 23068672 | tf_op jit(solution)/shard_map/dot_general | solution.py:203
  100.1 9.6 %multiply_convert_fusion.1 = bf16[1024,2048]{1,0:T(8,128)(2,1)S(1)} fusion(f32[1024,2048]{1,0:T(8,128)} %fusion.8, f32[1024,2048]{1,0:T(8,128)} %add_maximum_fusion, bf16[1024,1024]{1,0:T(8,128)(2,1)S(1)} %bitcast.24, bf16[2048,1024]{1,0:T(8,128)(2,1)} %get-tuple-element.10), kind=kOutput, calls=%fused_computation.3 | convolution fusion | flops 4303355904 | bytes 27262976 | tf_op jit(solution)/shard_map/dot_general | solution.py:22
  109.6 0.0 copy-start.1
  109.6 0.0 copy-start.7
  109.6 6.2 %convolution_convert_fusion.1 = bf16[1024,2048]{1,0:T(8,128)(2,1)} fusion(bf16[1024,1024]{1,0:T(8,128)(2,1)S(1)} %bitcast.27, bf16[1024,2048]{1,0:T(8,128)(2,1)S(1)} %multiply_convert_fusion.1), kind=kOutput, calls=%fused_computation.6 | convolution fusion | flops 4297064448 | bytes 10485760 | tf_op jit(solution)/shard_map/dot_general | solution.py:16
  115.9 0.0 copy-done.1
  115.9 0.0 collective-permute-start.1
  115.9 0.0 copy-done.7
  115.9 6.5 %convolution_convert_fusion = bf16[2048,1024]{1,0:T(8,128)(2,1)} fusion(bf16[1024,1024]{1,0:T(8,128)(2,1)S(1)} %bitcast.25, f32[1024,2048]{1,0:T(8,128)S(1)} %copy-done.7), kind=kOutput, calls=%fused_computation.5 | convolution fusion | flops 4301258752 | bytes 14680064 | tf_op jit(solution)/shard_map/dot_general | solution.py:16
  122.4 0.3 collective-permute-start.2
  122.7 4.0 %convolution_convert_fusion.3 = bf16[128,1024]{1,0:T(8,128)(2,1)S(1)} fusion(bf16[1024,2048]{1,0:T(8,128)(2,1)} %up_ref.1, bf16[1024,2048]{1,0:T(8,128)(2,1)} %copy-done.1, s32[]{:T(128)S(6)} %select_n.16), kind=kOutput, calls=%fused_computation.9 | convolution fusion | flops 537001984 | bytes 4980740 | tf_op jit(solution)/shard_map/dot_general | solution.py:22
  126.7 0.0 copy-done.2
  126.7 3.7 %broadcast_select_fusion = (bf16[128,1024]{1,0:T(8,128)(2,1)S(1)}, bf16[128,1024]{1,0:T(8,128)(2,1)S(1)}) fusion(bf16[128,1024]{1,0:T(8,128)(2,1)S(1)} %convolution_convert_fusion.3, pred[]{:T(512)S(6)} %eq.3, bf16[1024,2048]{1,0:T(8,128)(2,1)} %get-tuple-element.8, bf16[1024,2048]{1,0:T(8,128)(2,1)S(1)} %copy-done.2, s32[]{:T(128)S(6)} %select_n.16), kind=kOutput, calls=%fused_computation.13 | convolution fusion | flops 537133056 | bytes 5505029 | tf_op jit(solution)/shard_map/dot_general | solution.py:22
  130.4 1.5 collective-permute-start
  132.0 6.9 %collective-permute-done = bf16[128,1024]{1,0:T(8,128)(2,1)S(1)} collective-permute-done((bf16[128,1024]{1,0:T(8,128)(2,1)S(1)}, bf16[128,1024]{1,0:T(8,128)(2,1)S(1)}, u32[]{:S(2)}, u32[]{:S(2)}) %collective-permute-start) | collective-permute-done | bytes 262176 | tf_op jit(solution)/shard_map/ppermute | solution.py:193
  138.9 0.8 add_convert_fusion
  139.7 0.0 collective-permute-done.1
  139.7 9.0 %convert_add_fusion.1 = f32[1024,2048]{1,0:T(8,128)} fusion(bf16[1024,2048]{1,0:T(8,128)(2,1)} %collective-permute-done.1, bf16[1024,1024]{1,0:T(8,128)(2,1)S(1)} %bitcast.21, bf16[1024,2048]{1,0:T(8,128)(2,1)S(1)} %copy-done.2), kind=kOutput, calls=%fused_computation.2 | convolution fusion | flops 4299161600 | bytes 18874368 | tf_op jit(solution)/shard_map/dot_general | solution.py:16
  148.8 0.0 collective-permute-done.2
  148.8 0.0 slice-done
  148.8 0.0 copy-done.6
  148.8 8.5 %convert_add_fusion = f32[2048,1024]{1,0:T(8,128)} fusion(bf16[2048,1024]{1,0:T(8,128)(2,1)} %collective-permute-done.2, bf16[1024,1024]{1,0:T(8,128)(2,1)S(1)} %bitcast.23, f32[1024,2048]{1,0:T(8,128)S(1)} %bitcast.29), kind=kOutput, calls=%fused_computation | convolution fusion | flops 4303355904 | bytes 23068672 | tf_op jit(solution)/shard_map/dot_general | solution.py:16
  (8 shorter events, 0.0 us)
Async XLA Ops:
  77.2 4.7 %copy-start.3 = (bf16[2048,1024]{1,0:T(8,128)(2,1)S(1)}, bf16[2048,1024]{1,0:T(8,128)(2,1)}, u32[]{:S(2)}) copy-start(bf16[2048,1024]{1,0:T(8,128)(2,1)} %down_ref.1) | copy-start | bytes 12582916
  81.3 7.4 %copy-start.5 = (bf16[1,8,128,1024]{3,2,1,0:T(8,128)(2,1)}, bf16[1,8,128,1024]{3,2,1,0:T(8,128)(2,1)S(1)}, u32[]{:S(2)}) copy-start(bf16[1,8,128,1024]{3,2,1,0:T(8,128)(2,1)S(1)} %get-tuple-element.12) | copy-start | bytes 6291460
  81.9 6.8 %copy-start = (bf16[1024,2048]{1,0:T(8,128)(2,1)S(1)}, bf16[1024,2048]{1,0:T(8,128)(2,1)}, u32[]{:S(2)}) copy-start(bf16[1024,2048]{1,0:T(8,128)(2,1)} %up_ref.1) | copy-start | bytes 12582916
  88.7 4.5 %copy-start.4 = (bf16[1024,2048]{1,0:T(8,128)(2,1)S(1)}, bf16[1024,2048]{1,0:T(8,128)(2,1)}, u32[]{:S(2)}) copy-start(bf16[1024,2048]{1,0:T(8,128)(2,1)} %get-tuple-element.8) | copy-start | bytes 12582916
  109.6 6.3 %copy-start.1 = (bf16[1024,2048]{1,0:T(8,128)(2,1)}, bf16[1024,2048]{1,0:T(8,128)(2,1)S(1)}, u32[]{:S(2)}) copy-start(bf16[1024,2048]{1,0:T(8,128)(2,1)S(1)} %multiply_convert_fusion.1) | copy-start | bytes 12582916
  109.6 6.3 %copy-start.7 = (f32[1024,2048]{1,0:T(8,128)S(1)}, f32[1024,2048]{1,0:T(8,128)}, u32[]{:S(2)}) copy-start(f32[1024,2048]{1,0:T(8,128)} %add_maximum_fusion) | copy-start | bytes 25165828
  115.9 23.9 %collective-permute-start.1 = (bf16[1024,2048]{1,0:T(8,128)(2,1)}, bf16[1024,2048]{1,0:T(8,128)(2,1)}, u32[]{:S(2)}, u32[]{:S(2)}) collective-permute-start(bf16[1024,2048]{1,0:T(8,128)(2,1)} %convolution_convert_fusion.1), channel_id=1, source_target_pairs={{0,2},{2,0},{1,3},{3,1},{4,6},{6,4},{5,7},{7,5},{8,10},{10,8},{9,1... | collective-permute-start | bytes 12582920 | tf_op jit(solution)/shard_map/ppermute | solution.py:193
  122.4 26.4 %collective-permute-start.2 = (bf16[2048,1024]{1,0:T(8,128)(2,1)}, bf16[2048,1024]{1,0:T(8,128)(2,1)}, u32[]{:S(2)}, u32[]{:S(2)}) collective-permute-start(bf16[2048,1024]{1,0:T(8,128)(2,1)} %convolution_convert_fusion), channel_id=1, source_target_pairs={{0,2},{2,0},{1,3},{3,1},{4,6},{6,4},{5,7},{7,5},{8,10},{10,8},{9,1... | collective-permute-start | bytes 12582920 | tf_op jit(solution)/shard_map/ppermute | solution.py:193
  122.7 4.0 %copy-start.2 = (bf16[1024,2048]{1,0:T(8,128)(2,1)S(1)}, bf16[1024,2048]{1,0:T(8,128)(2,1)}, u32[]{:S(2)}) copy-start(bf16[1024,2048]{1,0:T(8,128)(2,1)} %copy-done.1) | copy-start | bytes 12582916
  130.4 8.5 %collective-permute-start = (bf16[128,1024]{1,0:T(8,128)(2,1)S(1)}, bf16[128,1024]{1,0:T(8,128)(2,1)S(1)}, u32[]{:S(2)}, u32[]{:S(2)}) collective-permute-start(bf16[128,1024]{1,0:T(8,128)(2,1)S(1)} %get-tuple-element.15), channel_id=1, source_target_pairs={{0,1},{1,0},{2,3},{3,2},{4,5},{5,4},{6,7},{7,6},{8,9},{9,8},{10,11... | collective-permute-start | bytes 786440 | tf_op jit(solution)/shard_map/ppermute | solution.py:193
  138.9 9.9 %slice-start = ((s8[8388608]{0:T(1024)(128)(4,1)}), s8[4194304]{0:T(1024)(128)(4,1)S(1)}, s32[]{:S(2)}) async-start(s8[8388608]{0:T(1024)(128)(4,1)} %bitcast.28), calls=%async_computation | async-start | bytes 8388608
  139.7 9.0 %copy-start.6 = (bf16[1,8,128,1024]{3,2,1,0:T(8,128)(2,1)S(1)}, bf16[1,8,128,1024]{3,2,1,0:T(8,128)(2,1)}, u32[]{:S(2)}) copy-start(bf16[1,8,128,1024]{3,2,1,0:T(8,128)(2,1)} %copy-done.5) | copy-start | bytes 6291460
  139.7 9.0 %slice-start.1 = ((s8[8388608]{0:T(1024)(128)(4,1)}), s8[4194304]{0:T(1024)(128)(4,1)S(1)}, s32[]{:S(2)}) async-start(s8[8388608]{0:T(1024)(128)(4,1)} %bitcast.28), calls=%async_computation.1 | async-start | bytes 8388608

commit v2 on v0

--- a/solution.py
+++ b/solution.py
@@ -1,7 +1,15 @@
+import functools
+
 import jax
 import jax.numpy as jnp
 from jax import lax
+from jax.experimental import pallas as pl
+from jax.experimental.pallas import tpu as pltpu
 from jax.sharding import PartitionSpec as P
+
+MESH = pl.DeviceIdType.MESH
+X, Y, UP, DOWN = range(4)
+PAIR = 2
 
 
 def contract_rows(left, right):
@@ -16,7 +24,281 @@
     )
 
 
-def shards(inputs, cotangent, w_up, w_down):
+def nearest(z, depth, index):
+    near = jnp.minimum(z, depth - 1 - z)
+    away = (index + 1) // 2
+    around = z - away if index % 2 else z + away
+    outward = jnp.where(z < depth - 1 - z, z + (index - near), z - (index - near))
+    return jnp.where(index <= 2 * near, around, outward)
+
+
+def hidden_kernel(reps, x_ref, c_ref, up_ref, down_ref,
+                  pg_out, sq_out, x_out, c_out, mine_out, theirs_out,
+                  gx, gc, up, down, pg, sq,
+                  send_sem, recv_sem, swap_sem, own_sem, pair_send, pair_recv, out_sem):
+    rep, fs, tp = lax.axis_index("rep"), lax.axis_index("fs"), lax.axis_index("tp")
+    z, y = rep // PAIR, rep % PAIR
+    depth = reps // PAIR
+    height = x_ref.shape[0]
+    half = height // 2
+    plane = PAIR * height
+    hidden = up.shape[2]
+    target = {
+        X: {"tp": 1 - tp},
+        Y: {"rep": z * PAIR + (1 - y)},
+        UP: {"rep": jnp.minimum(z + 1, depth - 1) * PAIR + y},
+        DOWN: {"rep": jnp.maximum(z - 1, 0) * PAIR + y},
+    }
+    sibling = {"fs": 1 - fs}
+
+    def when(condition, body):
+        if condition is True:
+            body()
+        else:
+            pl.when(condition)(body)
+
+    barrier = pltpu.get_barrier_semaphore()
+
+    def greet(device):
+        pl.semaphore_signal(barrier, inc=1, device_id=device, device_id_type=MESH)
+
+    greet(target[X])
+    greet(target[Y])
+    greet(sibling)
+    when(z < depth - 1, lambda: greet(target[UP]))
+    when(z > 0, lambda: greet(target[DOWN]))
+    pl.semaphore_wait(barrier, 3 + (z < depth - 1).astype(jnp.int32) + (z > 0).astype(jnp.int32))
+
+    def token(core, source, extra=0):
+        return pl.multiple_of((core * reps + source) * height + extra, half)
+
+    def copy(way, sub, at, own=False):
+        at_z, at_y, at_t = at
+        array, part = sub
+        source = at_z * PAIR + at_y
+        there = (gx, gc)[array].at[(at_t + fs) % 2, pl.ds(token(fs, source, part * half), half)]
+        here = (x_ref, c_ref)[array].at[pl.ds(part * half, half)] if own else there
+        index, piece = array * 2 + part, source * 2 + at_t
+        return pltpu.make_async_remote_copy(
+            src_ref=here, dst_ref=there,
+            send_sem=send_sem.at[way, index, piece],
+            recv_sem=recv_sem.at[index, piece],
+            device_id=target[way], device_id_type=MESH,
+        )
+
+    started, locals_started = [], []
+
+    def start(way, sub, at, condition=True, own=False):
+        when(condition, lambda: copy(way, sub, at, own).start())
+        started.append((way, sub, at, condition, own))
+
+    def arrive(sub, at):
+        copy(X, sub, at).wait_recv()
+
+    def put(here, there, sem):
+        moved = pltpu.make_async_copy(here, there, sem)
+        moved.start()
+        locals_started.append(moved)
+        return moved
+
+    subs = [(array, part) for part in range(2) for array in range(2)]
+    first = [(array, 0) for array in range(2)]
+    second = [(array, 1) for array in range(2)]
+    planes = [nearest(z, depth, index) for index in range(depth)]
+
+    here = (z, y, tp)
+    for sub in subs:
+        start(UP, sub, here, z < depth - 1, own=True)
+        start(DOWN, sub, here, z > 0, own=True)
+    for sub in first + second:
+        start(X, sub, here, own=True)
+    for sub in second + first:
+        start(Y, sub, here, own=True)
+    own_slot = (tp + fs) % 2
+    own_rows = pl.ds(token(fs, rep), height)
+    owns = [
+        pltpu.make_async_copy(from_ref, into, own_sem.at[index])
+        for index, (from_ref, into) in enumerate((
+            (x_ref, gx.at[own_slot, own_rows]), (c_ref, gc.at[own_slot, own_rows]),
+            (up_ref, up.at[0]), (down_ref, down.at[0]),
+        ))
+    ]
+    for own in owns:
+        own.start()
+    swaps = [
+        pltpu.make_async_remote_copy(
+            src_ref=from_ref, dst_ref=into.at[1], send_sem=swap_sem.at[0, index], recv_sem=swap_sem.at[1, index],
+            device_id=sibling, device_id_type=MESH,
+        )
+        for index, (from_ref, into) in enumerate(((up_ref, up), (down_ref, down)))
+    ]
+    for swap in swaps:
+        swap.start()
+
+    def from_z(index):
+        at_z = planes[index]
+        at = (at_z, y, tp)
+        for sub in subs:
+            arrive(sub, at)
+            start(UP, sub, at, jnp.logical_and(at_z < z, z < depth - 1))
+            start(DOWN, sub, at, jnp.logical_and(at_z > z, z > 0))
+        for sub in first + second:
+            start(X, sub, at)
+        for sub in second + first:
+            start(Y, sub, at)
+
+    def cross(index):
+        at_z = planes[index]
+        for one, two in zip(first, second):
+            across_x, across_y = (at_z, y, 1 - tp), (at_z, 1 - y, tp)
+            arrive(one, across_x)
+            start(Y, one, across_x)
+            arrive(two, across_y)
+            start(X, two, across_y)
+
+    def pair_copy(index, array, slot, core):
+        rows = pl.ds(token(core, planes[index] * PAIR), plane)
+        held = (gx, gc)[array]
+        return pltpu.make_async_remote_copy(
+            src_ref=held.at[slot, rows], dst_ref=held.at[1 - slot, rows],
+            send_sem=pair_send.at[array * 2 + slot, index], recv_sem=pair_recv.at[array * 2 + slot, index],
+            device_id=sibling, device_id_type=MESH,
+        )
+
+    quads = [(array, slot) for array in range(2) for slot in range(2)]
+
+    def keep(index, core, number):
+        rows = pl.ds(token(core, planes[index] * PAIR), plane)
+        put(gx.at[0, rows], x_out.at[rows], out_sem.at[0, number, index])
+        put(gc.at[0, rows], c_out.at[rows], out_sem.at[1, number, index])
+
+    def rest(index):
+        at_z = planes[index]
+        for one, two in zip(first, second):
+            arrive(one, (at_z, 1 - y, tp))
+            arrive(two, (at_z, y, 1 - tp))
+        for sub in subs:
+            arrive(sub, (at_z, 1 - y, 1 - tp))
+        for array, slot in quads:
+            pair_copy(index, array, slot, fs).start()
+        keep(index, fs, 0)
+
+    def compute(index, core, number):
+        rows = pl.ds(token(core, planes[index] * PAIR), plane)
+        tile = hidden // 4
+
+        @pl.loop(0, hidden // tile)
+        def _(step):
+            cols = pl.ds(pl.multiple_of(step * tile, tile), tile)
+            preact = (
+                jnp.dot(gx[0, rows, :], up[0, :, cols], preferred_element_type=jnp.float32)
+                + jnp.dot(gx[1, rows, :], up[1, :, cols], preferred_element_type=jnp.float32)
+            )
+            act_grad = contract_cols(gc[0, rows, :], down[0, cols, :]) + contract_cols(gc[1, rows, :], down[1, cols, :])
+            relu_pre = jnp.maximum(preact, 0.0)
+            sq[rows, cols] = (relu_pre * relu_pre).astype(sq.dtype)
+            pg[rows, cols] = (2.0 * relu_pre * act_grad).astype(pg.dtype)
+
+        put(pg.at[rows], pg_out.at[rows], out_sem.at[2, number, index])
+        put(sq.at[rows], sq_out.at[rows], out_sem.at[3, number, index])
+
+    def compute_other(index):
+        for array, slot in quads:
+            pair_copy(index, array, slot, 1 - fs).wait_recv()
+        keep(index, 1 - fs, 1)
+        compute(index, 1 - fs, 1)
+
+    def partial():
+        width = mine_out.shape[1]
+        tile = width // 4
+
+        @pl.loop(0, width // tile)
+        def _(step):
+            cols = pl.ds(pl.multiple_of(step * tile, tile), tile)
+            for slot, into in ((own_slot, mine_out), (1 - own_slot, theirs_out)):
+                into[:, cols] = contract_cols(pg[own_rows, :], up[slot, cols, :]).astype(into.dtype)
+
+    cross(0)
+    for index in range(1, min(3, depth)):
+        from_z(index)
+    for own in owns:
+        own.wait()
+    rest(0)
+    for swap in swaps:
+        swap.wait()
+    compute(0, fs, 0)
+    for index in range(3, depth):
+        from_z(index)
+    if depth > 1:
+        cross(1)
+    compute_other(0)
+    for index in range(2, depth):
+        cross(index)
+        rest(index - 1)
+        compute(index - 1, fs, 0)
+        if index == 2:
+            partial()
+        compute_other(index - 1)
+    if depth <= 2:
+        partial()
+    if depth > 1:
+        rest(depth - 1)
+        compute(depth - 1, fs, 0)
+        compute_other(depth - 1)
+    for way, sub, at, condition, own in started:
+        when(condition, lambda: copy(way, sub, at, own).wait_send())
+    for index in range(depth):
+        for array, slot in quads:
+            pair_copy(index, array, slot, fs).wait_send()
+    for moved in locals_started:
+        moved.wait()
+
+
+def hidden_gradients(reps, inputs, cotangent, w_up, w_down):
+    rows, cols = inputs.shape
+    hidden = w_up.shape[1]
+    tokens, depth = 2 * reps * rows, reps // PAIR
+    low = inputs.dtype
+    anywhere, vmem = pl.BlockSpec(memory_space=pl.ANY), pl.BlockSpec(memory_space=pltpu.VMEM)
+    whole, wide, part = (tokens, cols), (tokens, hidden), (rows, cols)
+    flops = 8 * tokens * cols * 2 * hidden
+    return pl.pallas_call(
+        functools.partial(hidden_kernel, reps),
+        out_shape=[jax.ShapeDtypeStruct(shape, low) for shape in (wide, wide, whole, whole, part, part)],
+        in_specs=[vmem, vmem, anywhere, anywhere],
+        out_specs=[anywhere] * 4 + [vmem] * 2,
+        scratch_shapes=[
+            pltpu.VMEM((2,) + whole, low),
+            pltpu.VMEM((2,) + whole, low),
+            pltpu.VMEM((2,) + w_up.shape, low),
+            pltpu.VMEM((2,) + w_down.shape, low),
+            pltpu.VMEM(wide, low),
+            pltpu.VMEM(wide, low),
+            pltpu.SemaphoreType.DMA((4, 4, reps * 2)),
+            pltpu.SemaphoreType.DMA((4, reps * 2)),
+            pltpu.SemaphoreType.DMA((2, 2)),
+            pltpu.SemaphoreType.DMA((4,)),
+            pltpu.SemaphoreType.DMA((4, depth)),
+            pltpu.SemaphoreType.DMA((4, depth)),
+            pltpu.SemaphoreType.DMA((4, 2, depth)),
+        ],
+        cost_estimate=pl.CostEstimate(flops=flops, bytes_accessed=tokens * hidden * 8, transcendentals=0),
+        compiler_params=pltpu.CompilerParams(
+            collective_id=0, has_side_effects=True, vmem_limit_bytes=60 * 1024 * 1024
+        ),
+    )(inputs, cotangent, w_up, w_down)
+
+
+def few_tokens(reps, inputs, cotangent, w_up, w_down):
+    pre_grad, squared, cols_in, cols_cot, mine, theirs = hidden_gradients(reps, inputs, cotangent, w_up, w_down)
+    theirs = lax.ppermute(theirs, "tp", [(0, 1), (1, 0)])
+    grad_up = contract_rows(cols_in, pre_grad)
+    grad_down = contract_rows(squared, cols_cot)
+    grad_inputs = (mine.astype(jnp.float32) + theirs.astype(jnp.float32)).astype(jnp.bfloat16)
+    return grad_inputs, grad_up, grad_down
+
+
+def many_tokens(inputs, cotangent, w_up, w_down):
     rows_in, rows_cot = (
         lax.all_gather(inputs, "tp", axis=1, tiled=True),
         lax.all_gather(cotangent, "tp", axis=1, tiled=True),
@@ -50,6 +332,16 @@
 
 
 def solution(mesh):
+    reps, n_fs, n_tp = mesh.shape["rep"], mesh.shape["fs"], mesh.shape["tp"]
+
+    def shards(inputs, cotangent, w_up, w_down):
+        gathered = 2 * reps * n_tp * inputs.size * inputs.dtype.itemsize
+        gradients = (w_up.size + w_down.size) * 4
+        fits = n_fs == 2 and n_tp == 2 and reps % PAIR == 0 and inputs.shape[0] % 32 == 0
+        if fits and gathered <= gradients:
+            return few_tokens(reps, inputs, cotangent, w_up, w_down)
+        return many_tokens(inputs, cotangent, w_up, w_down)
+
     return jax.shard_map(
         shards,
         mesh=mesh,

time: 670 us -> 132 us (0.20)
  waiting for transfers between devices: 579 us -> 0.01 us
  Pallas kernels: 0 us -> 103 us
  blocking collectives: 26.4 us -> 0 us
  local copies, waits for them, and re-layouts: 18.4 us -> 0.01 us
  between operations: 13.9 us -> 0.65 us
    reduce_scatter x3 -> x0, waiting for transfers between devices: 313 us -> none  [the longest x1 151 us: shards(): lax.psum_scatter(local_down, 'rep', scatter_dimension=0, tiled=True)]
    all_gather x6 -> x0, waiting for transfers between devices: 264 us -> none  [the longest x1 119 us: shards(): grad_up = lax.all_gather(slice_up, 'rep', axis=0, tiled=True)]
    pallas_call x0 -> x1, Pallas kernels: none -> 103 us  [hidden_gradients(): pl.pallas_call(functools.partial(hidden_kernel, reps), out_shape=[jax.Sha...]
    dot_general x3 -> x0, matrix products: 19.6 us -> none  [the longest x2 14.2 us: contract_cols(): lax.dot_general(left, right, (((1,), (1,)), ((), ())), preferred_element_...]
    all_gather x2 -> x0, blocking collectives: 18.1 us -> none  [the longest x1 9.94 us: shards(): lax.all_gather(inputs, 'tp', axis=1, tiled=True)]
    unnamed x10 -> x6, local copies, waits for them, and re-layouts: 18 us -> 0.01 us
    dot_general x2, matrix products: 11.9 us -> 26.3 us  [contract_rows(): lax.dot_general(left, right, (((0,), (0,)), ((), ())), preferred_element_...]
    all_to_all x2 -> x0, blocking collectives: 8.31 us -> none  [the longest x1 4.15 us: shards(): lax.all_to_all(rows_cot, 'fs', split_axis=1, concat_axis=0, tiled=True)]
  transfers between devices with their start and end apart: 9 -> 1, of which waited for: 9 -> 0; matrix products, arithmetic and copies ran while one was open for 5% -> 20% of each run, Pallas kernels for 0% -> 0%
where the time goes in v2:
time: 132 us
  Pallas kernels  103 us (78%)
  matrix products  26.3 us (20%)
  starting transfers between devices  1.55 us (1%)
    pallas_call x1, Pallas kernels, hidden_gradients(): pl.pallas_call(functools.partial(hidden_kernel, reps), out_shape=[jax.Sha...  103 us
    dot_general x2, matrix products, contract_rows(): lax.dot_general(left, right, (((0,), (0,)), ((), ())), preferred_element_...  26.3 us
  transfers between devices with their start and end apart: 1, of which 0 were waited for; matrix products, arithmetic and copies ran while one was open for 20% of the time, Pallas kernels for 0%

profile of v2, /device:TPU:0, one launch (start us, length us, event | category | flops | bytes accessed | tf_op | source)
XLA Modules:
  0.0 132.0 jit_solution(13817875109579514997)
XLA Ops:
  0.6 102.7 %shard_map.67 = (bf16[2048,2048]{1,0:T(8,128)(2,1)}, bf16[2048,2048]{1,0:T(8,128)(2,1)}, bf16[2048,1024]{1,0:T(8,128)(2,1)}, bf16[2048,1024]{1,0:T(8,128)(2,1)},...) custom-call(bf16[128,1024]{1,0:T(8,128)(2,1)} %x_ref.1, bf16[128,1024]{1,0:T(8,128)(2,1)} %c_ref.1, ...), custom_call_target="tpu_custom_call" | custom-call | flops 68719476736 | bytes 33554432 | tf_op jit(solution)/shard_map/pallas_call | solution.py:265
  103.3 1.6 %collective-permute-start = (bf16[128,1024]{1,0:T(8,128)(2,1)}, bf16[128,1024]{1,0:T(8,128)(2,1)S(1)}, u32[]{:S(2)}, u32[]{:S(2)}) collective-permute-start(bf16[128,1024]{1,0:T(8,128)(2,1)} %get-tuple-element.10), channel_id=1, source_target_pairs={{0,1},{1,0},{2,3},{3,2},{4,5},{5,4},{6,7},{7,6},{8,9},{9,8},{10,11... | collective-permute-start | bytes 786440 | tf_op jit(solution)/shard_map/ppermute | solution.py:294
  104.9 0.0 copy-start.1
  104.9 0.0 copy-start.2
  104.9 14.8 %fusion = f32[1024,2048]{1,0:T(8,128)} fusion(bf16[2048,1024]{1,0:T(8,128)(2,1)} %get-tuple-element.11, bf16[2048,2048]{1,0:T(8,128)(2,1)} %get-tuple-element.12), kind=kOutput, calls=%fused_computation.1 | convolution fusion | flops 8589934592 | bytes 20971520 | tf_op jit(solution)/shard_map/dot_general | solution.py:16
  119.6 0.0 copy-done.1
  119.6 0.0 copy-done.2
  119.6 0.0 copy-start
  119.6 11.6 %fusion.1 = f32[2048,1024]{1,0:T(8,128)} fusion(bf16[2048,2048]{1,0:T(8,128)(2,1)S(1)} %copy-done.1, bf16[2048,1024]{1,0:T(8,128)(2,1)S(1)} %copy-done.2), kind=kOutput, calls=%fused_computation.2 | convolution fusion | flops 8589934592 | bytes 20971520 | tf_op jit(solution)/shard_map/dot_general | solution.py:16
  131.2 0.0 collective-permute-done
  131.2 0.0 copy-done
  131.2 0.8 add_convert_fusion
Async XLA Ops:
  103.3 27.9 %collective-permute-start = (bf16[128,1024]{1,0:T(8,128)(2,1)}, bf16[128,1024]{1,0:T(8,128)(2,1)S(1)}, u32[]{:S(2)}, u32[]{:S(2)}) collective-permute-start(bf16[128,1024]{1,0:T(8,128)(2,1)} %get-tuple-element.10), channel_id=1, source_target_pairs={{0,1},{1,0},{2,3},{3,2},{4,5},{5,4},{6,7},{7,6},{8,9},{9,8},{10,11... | collective-permute-start | bytes 786440 | tf_op jit(solution)/shard_map/ppermute | solution.py:294
  104.9 14.8 %copy-start.1 = (bf16[2048,2048]{1,0:T(8,128)(2,1)S(1)}, bf16[2048,2048]{1,0:T(8,128)(2,1)}, u32[]{:S(2)}) copy-start(bf16[2048,2048]{1,0:T(8,128)(2,1)} %get-tuple-element.13) | copy-start | bytes 25165828
  104.9 14.8 %copy-start.2 = (bf16[2048,1024]{1,0:T(8,128)(2,1)S(1)}, bf16[2048,1024]{1,0:T(8,128)(2,1)}, u32[]{:S(2)}) copy-start(bf16[2048,1024]{1,0:T(8,128)(2,1)} %get-tuple-element.14) | copy-start | bytes 12582916
  119.6 11.6 %copy-start = (bf16[128,1024]{1,0:T(8,128)(2,1)S(1)}, bf16[128,1024]{1,0:T(8,128)(2,1)}, u32[]{:S(2)}) copy-start(bf16[128,1024]{1,0:T(8,128)(2,1)} %get-tuple-element.9) | copy-start | bytes 786436

commit v3 on v2

--- a/solution.py
+++ b/solution.py
@@ -233,9 +233,9 @@
         cross(1)
     compute_other(0)
     for index in range(2, depth):
-        cross(index)
         rest(index - 1)
         compute(index - 1, fs, 0)
+        cross(index)
         if index == 2:
             partial()
         compute_other(index - 1)

time: 132 us -> 132 us (level)
  no operation moved by 1% of the time
where the time goes in v3:
time: 132 us
  Pallas kernels  103 us (78%)
  matrix products  26.3 us (20%)
    pallas_call x1, Pallas kernels, hidden_gradients(): pl.pallas_call(functools.partial(hidden_kernel, reps), out_shape=[jax.Sha...  103 us
    dot_general x2, matrix products, contract_rows(): lax.dot_general(left, right, (((0,), (0,)), ((), ())), preferred_element_...  26.3 us
  transfers between devices with their start and end apart: 1, of which 0 were waited for; matrix products, arithmetic and copies ran while one was open for 20% of the time, Pallas kernels for 0%

profile of v3, /device:TPU:0, one launch (start us, length us, event | category | flops | bytes accessed | tf_op | source)
XLA Modules:
  0.0 131.8 jit_solution(3358375556223587038)
XLA Ops:
  0.6 103.4 %shard_map.67 = (bf16[2048,2048]{1,0:T(8,128)(2,1)}, bf16[2048,2048]{1,0:T(8,128)(2,1)}, bf16[2048,1024]{1,0:T(8,128)(2,1)}, bf16[2048,1024]{1,0:T(8,128)(2,1)},...) custom-call(bf16[128,1024]{1,0:T(8,128)(2,1)} %x_ref.1, bf16[128,1024]{1,0:T(8,128)(2,1)} %c_ref.1, ...), custom_call_target="tpu_custom_call" | custom-call | flops 68719476736 | bytes 33554432 | tf_op jit(solution)/shard_map/pallas_call | solution.py:265
  104.1 0.6 collective-permute-start
  104.7 0.0 copy-start.1
  104.7 0.0 copy-start.2
  104.7 14.8 %fusion = f32[1024,2048]{1,0:T(8,128)} fusion(bf16[2048,1024]{1,0:T(8,128)(2,1)} %get-tuple-element.11, bf16[2048,2048]{1,0:T(8,128)(2,1)} %get-tuple-element.12), kind=kOutput, calls=%fused_computation.1 | convolution fusion | flops 8589934592 | bytes 20971520 | tf_op jit(solution)/shard_map/dot_general | solution.py:16
  119.4 0.0 copy-done.1
  119.4 0.0 copy-done.2
  119.4 0.0 copy-start
  119.4 11.6 %fusion.1 = f32[2048,1024]{1,0:T(8,128)} fusion(bf16[2048,2048]{1,0:T(8,128)(2,1)S(1)} %copy-done.1, bf16[2048,1024]{1,0:T(8,128)(2,1)S(1)} %copy-done.2), kind=kOutput, calls=%fused_computation.2 | convolution fusion | flops 8589934592 | bytes 20971520 | tf_op jit(solution)/shard_map/dot_general | solution.py:16
  131.0 0.0 collective-permute-done
  131.0 0.0 copy-done
  131.0 0.8 add_convert_fusion
Async XLA Ops:
  104.1 26.9 %collective-permute-start = (bf16[128,1024]{1,0:T(8,128)(2,1)}, bf16[128,1024]{1,0:T(8,128)(2,1)S(1)}, u32[]{:S(2)}, u32[]{:S(2)}) collective-permute-start(bf16[128,1024]{1,0:T(8,128)(2,1)} %get-tuple-element.10), channel_id=1, source_target_pairs={{0,1},{1,0},{2,3},{3,2},{4,5},{5,4},{6,7},{7,6},{8,9},{9,8},{10,11... | collective-permute-start | bytes 786440 | tf_op jit(solution)/shard_map/ppermute | solution.py:294
  104.7 14.8 %copy-start.1 = (bf16[2048,2048]{1,0:T(8,128)(2,1)S(1)}, bf16[2048,2048]{1,0:T(8,128)(2,1)}, u32[]{:S(2)}) copy-start(bf16[2048,2048]{1,0:T(8,128)(2,1)} %get-tuple-element.13) | copy-start | bytes 25165828
  104.7 14.8 %copy-start.2 = (bf16[2048,1024]{1,0:T(8,128)(2,1)S(1)}, bf16[2048,1024]{1,0:T(8,128)(2,1)}, u32[]{:S(2)}) copy-start(bf16[2048,1024]{1,0:T(8,128)(2,1)} %get-tuple-element.14) | copy-start | bytes 12582916
  119.4 11.6 %copy-start = (bf16[128,1024]{1,0:T(8,128)(2,1)S(1)}, bf16[128,1024]{1,0:T(8,128)(2,1)}, u32[]{:S(2)}) copy-start(bf16[128,1024]{1,0:T(8,128)(2,1)} %get-tuple-element.9) | copy-start | bytes 786436
